TPU v7x, 32 devices: a whole 2x2x4 slice. The times are simulated.
32 devices in a mesh: ep: 8 (over z, x), tp: 4 (over y, core).
Axes of the slice: x: 2, y: 2, z: 4, core: 2. Of those that a mesh axis runs over, the one named last changes fastest.
Arguments:
- queries: bfloat16 [2048, 1024], P('ep', 'tp'), may hold values from -192 to 192
- keys_values: bfloat16 [2048, 512], P('ep', 'tp'), may hold values from -192 to 192
- log_gate_cum: float32 [16, 2048], P('tp'), as said below
- mix_weight: bfloat16 [1024, 2048], P('tp'), may hold values from -0.1875 to 0.1875
- mix_gain: float32 [2048], replicated, may hold values from 0.1 to 1.9
- moe_in: bfloat16 [6144, 2048], P(('ep', 'tp')), may hold values from -6 to 6
- moe_gain: float32 [2048], replicated, may hold values from 0.1 to 1.9
- routes: int32 [6144, 2], P(('ep', 'tp')), may hold values from 0 to 7, all different within a row; in each aligned block of 192 rows (0 to 191, 192 to 383, ...) at most 72 rows name the same one
- route_weight: float32 [6144, 2], P(('ep', 'tp')), may hold values from 0.25 to 2
- expert_gate: bfloat16 [8, 2048, 1024], P('ep', None, 'tp'), may hold values from -0.125 to 0.125
- expert_up: bfloat16 [8, 2048, 1024], P('ep', None, 'tp'), may hold values from -0.125 to 0.125
- expert_down: bfloat16 [8, 1024, 2048], P('ep', 'tp'), may hold values from -0.1875 to 0.1875
Outputs:
- mix_result: bfloat16 [2048, 2048], P(('ep', 'tp'))
- moe_result: bfloat16 [6144, 2048], P(('ep', 'tp'))
Inputs may be any that keep to these rules, and one draw needn't show every extreme that they name: `log_gate_cum`: along positions each head's values never rise. `routes`: each row names 2 different experts. Among the rows of one device no expert is named more than 72 times, and in every draw some device names some expert exactly 72 times.
All inputs are finite; a program needn't handle non-finite values.
Results may differ from a plain program's by a relative error of at most 0.013.
Values may be sent and summed in bfloat16 or wider, within the bound.
A program may use at most 128 MiB of HBM per device.

v0:
```python
from functools import partial
import math

import jax
import jax.numpy as jnp
from jax import lax
from jax.sharding import PartitionSpec as P

HEAD = 64


EPSILON = 1e-06
NEGATIVE = -1e30


def rms_scale(values, gain):
    widened = values.astype(jnp.float32)
    return widened * lax.rsqrt(jnp.mean(widened * widened, axis=-1, keepdims=True) + EPSILON) * gain


def slot_tables(route_block, experts, capacity):
    rows_here, top_picks = route_block.shape
    flat_routes = route_block.reshape(-1)
    onehot = (flat_routes[:, None] == jnp.arange(experts, dtype=jnp.int32)[None, :]).astype(
        jnp.int32
    )
    earlier = jnp.cumsum(onehot, axis=0) - onehot
    position = jnp.sum(earlier * onehot, axis=1)
    source_row = jnp.full((experts * capacity,), rows_here, jnp.int32)
    source_row = source_row.at[flat_routes * capacity + position].set(
        jnp.arange(rows_here * top_picks, dtype=jnp.int32) // top_picks
    )
    return (position.reshape(rows_here, top_picks), source_row)


def fold_update(grouped, query_pos, query_gate, key_block, key_gate, key_pos, running):
    running_max, row_total, summed = running
    scores = jnp.einsum(
        "tgrd,ngd->grtn", grouped, key_block[:, :, 0], preferred_element_type=jnp.float32
    ) * HEAD ** (-0.5)
    scores = scores + query_gate[..., None] - key_gate[:, :, None, :]
    causal = key_pos[None, :] <= query_pos[:, None]
    scores = jnp.where(causal, scores, NEGATIVE)
    new_max = jnp.maximum(running_max, jnp.max(scores, axis=-1))
    factor = jnp.exp(running_max - new_max)
    weight = jnp.where(causal, jnp.exp(scores - new_max[..., None]), 0.0)
    row_total = row_total * factor + jnp.sum(weight, axis=-1)
    summed = summed * factor[..., None] + jnp.einsum(
        "grtn,ngd->grtd",
        weight.astype(jnp.bfloat16),
        key_block[:, :, 1],
        preferred_element_type=jnp.float32,
    )
    return (new_max, row_total, summed)


def keep_state(running):
    return running


def gated_hidden(slot_rows, router_feature_lanes, up_columns):
    return (
        jax.nn.silu(jnp.dot(slot_rows, router_feature_lanes, preferred_element_type=jnp.float32))
        * jnp.dot(slot_rows, up_columns, preferred_element_type=jnp.float32)
    ).astype(jnp.bfloat16)


def body(
    queries,
    keys_values,
    log_gate_cum,
    mix_weight,
    mix_gain,
    moe_in,
    moe_gain,
    routes,
    route_weight,
    expert_gate,
    expert_up,
    expert_down,
):
    ep_count = lax.axis_size("ep")
    ep_index = lax.axis_index("ep")
    local_tokens = queries.shape[0]
    half_rows = local_tokens // 2
    offset = ep_index * local_tokens
    kv_local = keys_values.shape[1] // (2 * HEAD)
    heads_local = queries.shape[1] // HEAD
    group_size = heads_local // kv_local
    second_rows = queries[half_rows:]
    second_start = offset + half_rows

    def half_setup(rows, first_pos):
        grouped = rows.reshape(half_rows, kv_local, group_size, HEAD)
        query_pos = first_pos + jnp.arange(half_rows, dtype=jnp.int32)
        query_gate = lax.dynamic_slice_in_dim(log_gate_cum, first_pos, half_rows, 1)
        query_gate = query_gate.reshape(kv_local, group_size, half_rows)
        return (grouped, query_pos, query_gate, first_pos + half_rows - 1)

    halves = (half_setup(queries[:half_rows], offset), half_setup(second_rows, second_start))
    start_state = (
        jnp.full((kv_local, group_size, half_rows), NEGATIVE, jnp.float32),
        jnp.zeros((kv_local, group_size, half_rows), jnp.float32),
        jnp.zeros((kv_local, group_size, half_rows, HEAD), jnp.float32),
    )
    piece = lax.all_gather(keys_values, "ep", axis=0, tiled=True)
    piece_rows = piece.shape[0]
    block_rows = math.gcd(piece_rows, 512)

    def one_block(turn_index, fold_state):
        tile_opening = turn_index * block_rows
        key_block = lax.dynamic_slice_in_dim(piece, turn_index * block_rows, block_rows, 0)
        key_block = key_block.reshape(block_rows, kv_local, 2, HEAD)
        key_gate = lax.dynamic_slice_in_dim(log_gate_cum, tile_opening, block_rows, 1)
        key_gate = key_gate.reshape(kv_local, group_size, block_rows)
        key_pos = tile_opening + jnp.arange(block_rows, dtype=jnp.int32)
        updated = []
        for half_state, half_data in zip(fold_state, halves):
            grouped, query_pos, query_gate, last_query = half_data
            advance = partial(
                fold_update, grouped, query_pos, query_gate, key_block, key_gate, key_pos
            )
            updated.append(lax.cond(tile_opening <= last_query, advance, keep_state, half_state))
        return tuple(updated)

    folded = lax.fori_loop(0, piece_rows // block_rows, one_block, (start_state, start_state))

    def finish(state):
        _, row_total, summed = state
        mixed_heads = jnp.transpose(summed / row_total[..., None], (2, 0, 1, 3))
        return mixed_heads.reshape(half_rows, heads_local * HEAD).astype(jnp.bfloat16)

    first_done = finish(folded[0])
    second_done = finish(folded[1])
    attended = jnp.concatenate([first_done, second_done], axis=0)
    rows_here = moe_in.shape[0]
    top_picks = routes.shape[1]
    width_here = moe_in.shape[1]
    capacity = 3 * top_picks * rows_here // (2 * ep_count)
    normed = rms_scale(moe_in, moe_gain).astype(jnp.bfloat16)
    position, source_row = slot_tables(routes, ep_count, capacity)
    zero_row = jnp.zeros((1, width_here), jnp.bfloat16)
    down_here = expert_down[0]
    padded = jnp.concatenate([normed, zero_row], axis=0)
    received_rows = lax.all_to_all(
        padded[source_row].reshape(ep_count, capacity, width_here),
        "ep",
        split_axis=0,
        concat_axis=0,
        tiled=True,
    )
    slot_rows = received_rows.reshape(-1, width_here)
    slot_count = slot_rows.shape[0]
    columns = gated_hidden(
        slot_rows,
        lax.all_gather(expert_gate[0], "tp", axis=1, tiled=True),
        lax.all_gather(expert_up[0], "tp", axis=1, tiled=True),
    )
    hidden = columns
    shard_rows = down_here.shape[0]
    total = jnp.zeros((slot_count, width_here), jnp.float32)
    add_piece = lax.all_gather(down_here, "tp", axis=0, tiled=True)
    for part_index in range(add_piece.shape[0] // shard_rows):
        columns = lax.dynamic_slice_in_dim(hidden, part_index * shard_rows, shard_rows, 1)
        width_part = jnp.dot(
            columns,
            add_piece[part_index * shard_rows : (part_index + 1) * shard_rows],
            preferred_element_type=jnp.float32,
        ).astype(jnp.bfloat16)
        total = total + lax.optimization_barrier(width_part).astype(jnp.float32)
    mix_sum = lax.psum_scatter(
        jnp.dot(attended, mix_weight, preferred_element_type=jnp.float32).astype(jnp.bfloat16),
        "tp",
        scatter_dimension=0,
        tiled=True,
    ).astype(jnp.float32)
    mix_result = rms_scale(mix_sum, mix_gain).astype(jnp.bfloat16)
    expert_out = total.astype(jnp.bfloat16).reshape(ep_count, capacity, width_here)
    returned = lax.all_to_all(expert_out, "ep", split_axis=0, concat_axis=0, tiled=True).reshape(
        -1, width_here
    )
    chosen = returned[routes * capacity + position].astype(jnp.float32)
    moe_result = jnp.sum(route_weight[..., None] * chosen, axis=1).astype(jnp.bfloat16)
    return (mix_result, moe_result)


def solution(mesh):
    in_specs = (
        P("ep", "tp"),
        P("ep", "tp"),
        P("tp", None),
        P("tp", None),
        P(),
        P(("ep", "tp"), None),
        P(),
        P(("ep", "tp"), None),
        P(("ep", "tp"), None),
        P("ep", None, "tp"),
        P("ep", None, "tp"),
        P("ep", "tp", None),
    )
    out_specs = (P(("ep", "tp"), None), P(("ep", "tp"), None))
    return jax.shard_map(body, mesh=mesh, in_specs=in_specs, out_specs=out_specs, check_vma=False)
```

profile of v0, /device:TPU:0, one launch (start us, length us, event | category | flops | bytes accessed | tf_op | source)
XLA Modules:
  0.0 230.8 jit_solution(3829767703458338959)
XLA Ops:
  7.3 0.7 all-gather.7.cloned.1.call-update
  8.0 0.7 all-gather.9.cloned.1.call-update
  8.7 0.7 all-gather.11.cloned.1.call-update
  9.9 0.9 reduce-window.6
  11.2 0.7 compare_select_fusion
  12.0 0.2 fusion.48
  12.3 0.3 fusion.50
  12.7 2.9 %scatter_custom_fusion = s32[576]{0:T(1024)S(1)} fusion(s32[384]{0:T(512)S(1)} %fusion.69, s32[384]{0:T(512)S(1)} %add_select_fusion, s32[]{:T(128)} %constant.112.clone.1), kind=kCustom, calls=%fused_computation.114 | custom fusion | bytes 2308 | tf_op jit(solution)/shard_map/scatter | solution.py:30
  15.6 4.0 %gather_fusion = bf16[576,2048]{1,0:T(8,128)(2,1)} fusion(bf16[193,2048]{1,0:T(8,128)(2,1)S(1)} %concatenate.7, s32[1024]{0:T(1024)S(1)} %pad_clamp_fusion.1), kind=kCustom, calls=%fused_computation | custom fusion | bytes 4720896 | tf_op jit(solution)/shard_map/gather | solution.py:146
  19.7 7.3 %all-to-all-start = ((bf16[8,72,2048]{2,1,0:T(8,128)(2,1)}), bf16[8,72,2048]{2,1,0:T(8,128)(2,1)S(1)}, u32[]{:S(2)}, u32[]{:S(2)}) async-start(bf16[8,72,2048]{2,1,0:T(8,128)(2,1)} %bitcast.137), calls=%async_computation.1 | async-start | bytes 4718592 | tf_op jit(solution)/shard_map/all_to_all | solution.py:145
  27.0 0.9 fusion.73
  27.8 0.7 copy.23
  28.6 0.7 copy.24
  29.3 0.9 copy.22
  30.2 1.3 constant_dynamic-slice_fusion.2
  31.5 72.5 %all_gather.12 = bf16[2048,128]{0,1:T(8,128)(2,1)} all-gather(bf16[256,128]{0,1:T(8,128)(2,1)S(1)} %copy.22), channel_id=1, replica_groups=mesh['ep'=8,'tp'=4] {'ep'}, dimensions={0}, use_global_device_ids=true | all-gather | bytes 589824 | tf_op jit(solution)/shard_map/all_gather | solution.py:106
  104.0 6.3 %fusion.44 = f32[576,1024]{1,0:T(8,128)} fusion(bf16[576,2048]{1,0:T(8,128)(2,1)S(1)} %bitcast.138, bf16[1,2048,1024]{2,1,0:T(8,128)(2,1)} %all-gather.7.cloned.1.call-done), kind=kOutput, calls=%fused_computation.63 | convolution fusion | flops 2415919104 | bytes 8912896 | tf_op jit(solution)/shard_map/dot_general | solution.py:63
  110.3 6.4 %multiply_convert_fusion = bf16[576,1024]{1,0:T(8,128)(2,1)} fusion(f32[576,1024]{1,0:T(8,128)} %fusion.44, bf16[576,2048]{1,0:T(8,128)(2,1)S(1)} %bitcast.139, bf16[1,2048,1024]{2,1,0:T(8,128)(2,1)} %all-gather.9.cloned.1.call-done), kind=kOutput, calls=%fused_computation.71 | convolution fusion | flops 2419458048 | bytes 10092544 | tf_op jit(solution)/shard_map/dot_general | solution.py:64
  116.7 3.3 %all-gather.11.cloned.1.call-done = bf16[1,1024,2048]{2,1,0:T(8,128)(2,1)} async-done(((bf16[1,256,2048]{2,1,0:T(8,128)(2,1)}), bf16[1,1024,2048]{2,1,0:T(8,128)(2,1)}) %all-gather.11.cloned.1.call-update) | async-done | bytes 4194320 | tf_op jit(solution)/shard_map/all_gather | solution.py:162
  120.0 2.2 convolution_convert_fusion.3
  122.2 2.0 convolution_convert_fusion.2
  124.3 0.8 convolution_convert_fusion.1
  125.1 0.8 convolution_convert_fusion
  125.8 3.5 %add_convert_fusion = bf16[576,2048]{1,0:T(8,128)(2,1)} fusion(bf16[576,2048]{1,0:T(8,128)(2,1)S(1)} %convolution_convert_fusion, bf16[576,2048]{1,0:T(8,128)(2,1)S(1)} %convolution_convert_fusion.1, bf16[576,2048]{1,0:T(8,128)(2,1)S(1)} %convolution_convert_fusion.2, bf16[576,2048]{1,0:T(8,128)(2,1)S(1)} %convolution_convert_fusion.3), kind=kLoop, calls=%fused_computation.60 | loop fusion | flops 9437184 | bytes 11796480 | tf_op jit(solution)/shard_map/convert_element_type | solution.py:178
  129.4 5.5 %all-to-all-start.1 = ((bf16[8,72,2048]{2,1,0:T(8,128)(2,1)}), bf16[8,72,2048]{2,1,0:T(8,128)(2,1)S(1)}, u32[]{:S(2)}, u32[]{:S(2)}) async-start(bf16[8,72,2048]{2,1,0:T(8,128)(2,1)} %bitcast.136), calls=%async_computation.2 | async-start | bytes 4718592 | tf_op jit(solution)/shard_map/all_to_all | solution.py:179
  134.9 0.3 reduce-scatter.2.cloned.1.call-start
  135.2 0.7 broadcast_in_dim.60
  135.8 0.7 broadcast_in_dim.60.clone
  136.5 0.6 broadcast_in_dim.59.clone
  137.1 20.5 %while.24 = (s32[]{:T(128)}, f32[1,4,128]{2,1,0:T(4,128)S(1)}, f32[1,4,128]{2,1,0:T(4,128)S(1)}, f32[1,4,128,64]{2,3,1,0:T(8,128)}, f32[1,4,128]{2,1,0:T(4,128)S...) while((s32[]{:T(128)}, f32[1,4,128]{2,1,0:T(4,128)S(1)}, ...), condition=%wide.region_9.10_spmd.clone, body=%wide.region_0.9_spmd.clone.sunk | while | flops 140250880 | bytes 10222291 | solution.py:126
  137.1 0.9 constant_dynamic-slice_fusion.6
  138.0 1.3 constant_dynamic-slice_fusion.7
  139.3 0.6 iota.57
  139.9 3.4 %conditional.7 = ((f32[1,4,128]{2,1,0:T(4,128)S(1)}, f32[1,4,128]{2,1,0:T(4,128)}, f32[1,4,128,64]{2,3,1,0:T(8,128)})) conditional(s32[]{:T(128)} %convert_element_type.168, (f32[1,4,128]{2,1,0:T(4,128)S(1)}, f32[1,4,128]{2,1,0:T(4,128)}, f32[1,4,128,64]{2,3,1,0:T(8,128)}) %tuple.67, (s32[512]{0:T(512)S(1)}, s32[]{:T(128)}, ...), branch_computations={%region_5.5_spmd, %region_6.8_spmd} | conditional | flops 70125184 | bytes 4978324 | solution.py:123
  139.9 0.7 broadcast_add_fusion.1
  140.7 1.3 fusion.72
  142.3 0.3 fusion.27
  142.6 0.6 copy-done.4
  143.3 0.6 iota.56
  143.9 3.4 %conditional.6 = ((f32[1,4,128]{2,1,0:T(4,128)S(1)}, f32[1,4,128]{2,1,0:T(4,128)S(1)}, f32[1,4,128,64]{2,3,1,0:T(8,128)})) conditional(s32[]{:T(128)} %convert_element_type.167, (f32[1,4,128]{2,1,0:T(4,128)S(1)}, f32[1,4,128]{2,1,0:T(4,128)S(1)}, f32[1,4,128,64]{2,3,1,0:T(8,128)}) %tuple.65, (s32[512]{0:T(512)S(1)}, s32[]{:T(128)}, ...), branch_computations={%region_1.0_spmd, %region_2.4_spmd} | conditional | flops 70125184 | bytes 4961884 | solution.py:123
  143.9 0.7 broadcast_add_fusion
  144.8 1.3 fusion.71
  146.3 0.3 fusion.8
  146.6 0.6 copy-done.2
  147.3 0.9 constant_dynamic-slice_fusion.6
  148.2 1.3 constant_dynamic-slice_fusion.7
  149.5 0.6 iota.57
  150.1 0.6 iota.56
  150.7 0.9 constant_dynamic-slice_fusion.6
  151.6 1.3 constant_dynamic-slice_fusion.7
  152.9 0.6 iota.57
  153.5 0.6 iota.56
  154.1 0.9 constant_dynamic-slice_fusion.6
  155.0 1.3 constant_dynamic-slice_fusion.7
  156.3 0.6 iota.57
  156.9 0.6 iota.56
  157.5 1.0 divide_convert_fusion
  158.6 1.4 convolution_convert_fusion.4
  160.3 45.4 %reduce-scatter.2.cloned.1.call-done = bf16[64,2048]{1,0:T(8,128)(2,1)} async-done(((bf16[256,2048]{1,0:T(8,128)(2,1)}), bf16[64,2048]{1,0:T(8,128)(2,1)}) %reduce-scatter.2.cloned.1.call-update) | async-done | bytes 262160 | tf_op jit(solution)/shard_map/reduce_scatter | solution.py:171
  205.7 1.1 fusion.51
  206.8 1.8 fusion.53
  208.6 3.1 %gather_fusion.1 = bf16[384,2048]{1,0:T(8,128)(2,1)} fusion(bf16[576,2048]{1,0:T(8,128)(2,1)S(1)} %bitcast.133, s32[1024]{0:T(1024)S(1)} %pad_clamp_fusion), kind=kCustom, calls=%fused_computation.1 | custom fusion | bytes 3147264 | tf_op jit(solution)/shard_map/gather | solution.py:182
  211.7 4.7 %reshape.219 = f32[192,2,2048]{2,1,0:T(2,128)} reshape(bf16[384,2048]{1,0:T(8,128)(2,1)} %gather_fusion.1) | data formatting | bytes 4718592 | tf_op jit(solution)/shard_map/convert_element_type | solution.py:182
  216.5 7.8 %multiply_reduce_fusion = bf16[192,2048]{1,0:T(8,128)(2,1)} fusion(f32[192,2,2048]{2,1,0:T(2,128)} %reshape.219, f32[192,2]{1,0:T(8,128)S(1)} %copy.25), kind=kLoop, calls=%fused_computation.65 | loop fusion | flops 1179648 | bytes 3933696 | tf_op jit(solution)/shard_map/reduce_sum | solution.py:183
  (78 shorter events, 2.4 us)
Async XLA Ops:
  7.2 151.4 %copy-start = (bf16[256,2048]{1,0:T(8,128)(2,1)S(1)}, bf16[256,2048]{1,0:T(8,128)(2,1)}, u32[]{:S(2)}) copy-start(bf16[256,2048]{1,0:T(8,128)(2,1)} %param.21) | copy-start | bytes 3145732
  7.2 2.3 copy-start.13
  7.2 4.8 %copy-start.6 = (bf16[192,2048]{1,0:T(8,128)(2,1)S(1)}, bf16[192,2048]{1,0:T(8,128)(2,1)}, u32[]{:S(2)}) copy-start(bf16[192,2048]{1,0:T(8,128)(2,1)} %param.23) | copy-start | bytes 2359300
  7.2 5.1 %copy-start.11 = (f32[2048]{0:T(1024)S(1)}, f32[2048]{0:T(1024)}, u32[]{:S(2)}) copy-start(f32[2048]{0:T(1024)} %param.24) | copy-start | bytes 24580
  7.2 96.8 %all-gather.7.cloned.1.call-start = ((), (), s32[]{:S(2)}) async-start(), calls=%async_computation.4 | async-start | bytes 5242880 | tf_op jit(solution)/shard_map/all_gather | solution.py:156
  7.9 102.3 %all-gather.9.cloned.1.call-start = ((), (), s32[]{:S(2)}) async-start(), calls=%async_computation.5 | async-start | bytes 5242880 | tf_op jit(solution)/shard_map/all_gather | solution.py:157
  8.7 111.3 %all-gather.11.cloned.1.call-start = ((), (), s32[]{:S(2)}) async-start(), calls=%async_computation.6 | async-start | bytes 5242880 | tf_op jit(solution)/shard_map/all_gather | solution.py:162
  19.7 84.3 %all-to-all-start = ((bf16[8,72,2048]{2,1,0:T(8,128)(2,1)}), bf16[8,72,2048]{2,1,0:T(8,128)(2,1)S(1)}, u32[]{:S(2)}, u32[]{:S(2)}) async-start(bf16[8,72,2048]{2,1,0:T(8,128)(2,1)} %bitcast.137), calls=%async_computation.1 | async-start | bytes 4718592 | tf_op jit(solution)/shard_map/all_to_all | solution.py:145
  116.7 5.5 %copy-start.7 = (bf16[576,1024]{1,0:T(8,128)(2,1)S(1)}, bf16[576,1024]{1,0:T(8,128)(2,1)}, u32[]{:S(2)}) copy-start(bf16[576,1024]{1,0:T(8,128)(2,1)} %multiply_convert_fusion) | copy-start | bytes 3538948
  120.0 4.3 %copy-start.5 = (bf16[1,1024,2048]{2,1,0:T(8,128)(2,1)S(1)}, bf16[1,1024,2048]{2,1,0:T(8,128)(2,1)}, u32[]{:S(2)}) copy-start(bf16[1,1024,2048]{2,1,0:T(8,128)(2,1)} %all-gather.11.cloned.1.call-done) | copy-start | bytes 12582916
  129.4 79.2 %all-to-all-start.1 = ((bf16[8,72,2048]{2,1,0:T(8,128)(2,1)}), bf16[8,72,2048]{2,1,0:T(8,128)(2,1)S(1)}, u32[]{:S(2)}, u32[]{:S(2)}) async-start(bf16[8,72,2048]{2,1,0:T(8,128)(2,1)} %bitcast.136), calls=%async_computation.2 | async-start | bytes 4718592 | tf_op jit(solution)/shard_map/all_to_all | solution.py:179
  134.9 70.8 %reduce-scatter.2.cloned.1.call-start = ((), (), s32[]{:S(2)}) async-start(), calls=%async_computation.3 | async-start | bytes 1310720 | tf_op jit(solution)/shard_map/reduce_scatter | solution.py:171
  139.9 2.4 %copy-start.9 = (f32[1,4,128]{2,1,0:T(4,128)S(1)}, f32[1,4,128]{2,1,0:T(4,128)}, u32[]{:S(2)}) copy-start(f32[1,4,128]{2,1,0:T(4,128)} %get-tuple-element.331) | copy-start | bytes 6148 | tf_op jit(solution)/shard_map/while/body/eval_jaxpr/cond
  139.9 2.4 %copy-start.3 = (f32[1,4,128,64]{2,3,1,0:T(8,128)S(1)}, f32[1,4,128,64]{2,3,1,0:T(8,128)}, u32[]{:S(2)}) copy-start(f32[1,4,128,64]{2,3,1,0:T(8,128)} %get-tuple-element.332) | copy-start | bytes 393220 | tf_op jit(solution)/shard_map/while/body/eval_jaxpr/cond
  142.3 1.0 copy-start.10
  142.6 0.7 copy-start.4
  143.9 2.4 %copy-start.1 = (f32[1,4,128,64]{2,3,1,0:T(8,128)S(1)}, f32[1,4,128,64]{2,3,1,0:T(8,128)}, u32[]{:S(2)}) copy-start(f32[1,4,128,64]{2,3,1,0:T(8,128)} %get-tuple-element.323) | copy-start | bytes 393220 | tf_op jit(solution)/shard_map/while/body/eval_jaxpr/cond
  146.6 0.7 copy-start.2
  157.5 2.5 %copy-start.8 = (s32[192,2]{1,0:T(8,128)S(1)}, s32[192,2]{1,0:T(8,128)}, u32[]{:S(2)}) copy-start(s32[192,2]{1,0:T(8,128)} %get-tuple-element.462) | copy-start | bytes 4612
  157.5 2.7 %copy-start.14 = (f32[192,2]{0,1:T(2,128)S(1)}, f32[192,2]{0,1:T(2,128)}, u32[]{:S(2)}) copy-start(f32[192,2]{0,1:T(2,128)} %param.26) | copy-start | bytes 4612
  157.5 49.3 %copy-start.12 = (f32[2048]{0:T(1024)S(1)}, f32[2048]{0:T(1024)}, u32[]{:S(2)}) copy-start(f32[2048]{0:T(1024)} %param.22) | copy-start | bytes 24580
Sparse Core Ops, SparseCore 0:
  9.6 37.7 all-gather.6
  48.9 34.9 all-gather.8
  85.5 34.4 all-gather.10
  160.2 45.4 reduce-scatter.1
where the time goes:
time: 232 us; the launch traced here: 231 us
  blocking collectives  72.5 us (31%)
  waiting for transfers between devices  50.7 us (22%)
  local copies, waits for them, and re-layouts  37.5 us (16%)
  matrix products  23.2 us (10%)
  other arithmetic  19.6 us (8%)
  between operations  14 us (6%)
  starting transfers between devices  13.2 us (6%)
    all_gather x1, blocking collectives, body(): piece = lax.all_gather(keys_values, 'ep', axis=0, tiled=True)  72.5 us
    reduce_scatter x1, waiting for transfers between devices, body(): lax.psum_scatter(jnp.dot(attended, mix_weight, preferred_element_type=jnp...  45.4 us
    reduce_sum x1, other arithmetic, body(): jnp.sum(route_weight[..., None] * chosen, axis=1).astype(jnp.bfloat16)  7.76 us
    all_to_all x1, starting transfers between devices, body(): lax.all_to_all(padded[source_row].reshape(ep_count, capacity, width_here)...  7.28 us
    dot_general x1, matrix products, gated_hidden(): jnp.dot(slot_rows, up_columns, preferred_element_type=jnp.float32)  6.42 us
    dot_general x1, matrix products, gated_hidden(): jnp.dot(slot_rows, router_feature_lanes, preferred_element_type=jnp.float32)  6.26 us
    dot_general x4, matrix products, body(): jnp.dot(columns, add_piece[part_index * shard_rows:(part_index + 1) * sha...  5.82 us
    all_to_all x1, starting transfers between devices, body(): lax.all_to_all(expert_out, 'ep', split_axis=0, concat_axis=0, tiled=True)  5.51 us
  transfers between devices with their start and end apart: 6, of which 2 were waited for; matrix products, arithmetic and copies ran while one was open for 23% of the time, Pallas kernels for 0%

commit v1 on v0

v1 whole, which is shorter than its diff:
```python
from functools import partial

import jax
import jax.numpy as jnp
from jax import lax
from jax.experimental import pallas as pl
from jax.experimental.pallas import tpu as pltpu
from jax.sharding import PartitionSpec as P

HEAD = 64
EPSILON = 1e-06
NEGATIVE = -1e30
MESH = pl.DeviceIdType.MESH
F32 = jnp.float32
BF16 = jnp.bfloat16


def round_up(value, unit):
    return -(-value // unit) * unit


def dot(a, b):
    return jnp.dot(a, b, preferred_element_type=F32)


def iota(shape, dim):
    return lax.broadcasted_iota(jnp.int32, shape, dim)


def rms_scale(widened, gain):
    return widened * lax.rsqrt(jnp.mean(widened * widened, axis=-1, keepdims=True) + EPSILON) * gain


def kernel(
    sizes,
    q_ref,
    kv_ref,
    key_gate_ref,
    query_gate_ref,
    mixw_ref,
    mix_gain_ref,
    x_ref,
    x_gain_ref,
    routes_ref,
    routes_t_ref,
    route_weight_ref,
    gate_hbm,
    up_hbm,
    down_hbm,
    mix_out,
    moe_out,
    gate_all,
    up_all,
    down_all,
    send_x,
    recv_x,
    hidden,
    send_y,
    recv_y,
    kv_all,
    q_pad,
    top,
    total,
    summed,
    mix_send,
    mix_recv,
    local_sem,
    far_send,
    far_recv,
    own_send,
    own_recv,
    fwd_send,
    fwd_recv,
    x_send_sem,
    x_recv_sem,
    kv_send_sem,
    kv_recv_sem,
    y_send_sem,
    y_recv_sem,
    mix_send_sem,
    mix_recv_sem,
):
    ep, tp, slot_rows, wire_rows, chunks = sizes
    me = lax.axis_index("ep")
    tme = lax.axis_index("tp")
    far = lax.rem(tme + tp // 2, tp)
    near = tme + 1 - 2 * lax.rem(tme, 2)
    near_far = lax.rem(near + tp // 2, tp)
    rows, width = x_ref.shape
    picks = routes_ref.shape[1]
    slots = ep * slot_rows
    shard = down_hbm.shape[1]
    cols = width // chunks
    tokens = q_ref.shape[0]
    heads = query_gate_ref.shape[1]
    kv_local = kv_ref.shape[1] // (2 * HEAD)
    group = heads // kv_local

    def weight_view(item, block):
        if item == 0:
            return gate_all.at[block]
        if item == 1:
            return up_all.at[block]
        return down_all.at[item - 2, pl.ds(pl.multiple_of(block * shard, shard), shard)]

    def weight_source(item):
        if item == 0:
            return gate_hbm.at[0]
        if item == 1:
            return up_hbm.at[0]
        return down_hbm.at[0, :, pl.ds((item - 2) * cols, cols)]

    items = 2 + chunks
    loads = [
        pltpu.make_async_copy(weight_source(i), weight_view(i, tme), local_sem.at[i])
        for i in range(items)
    ]
    for load in loads:
        load.start()
    recv_x[...] = jnp.zeros_like(recv_x)
    recv_y[...] = jnp.zeros_like(recv_y)

    barrier = pltpu.get_barrier_semaphore()

    def greet(step, carry):
        pl.semaphore_signal(
            barrier, inc=1, device_id={"ep": lax.rem(me + step, ep)}, device_id_type=MESH
        )
        return carry

    lax.fori_loop(1, ep, greet, 0)
    for step in range(1, tp):
        pl.semaphore_signal(
            barrier, inc=1, device_id={"tp": lax.rem(tme + step, tp)}, device_id_type=MESH
        )
    pl.semaphore_wait(barrier, ep - 1 + tp - 1)

    def weight_copy(item, block, target, send_sem, recv_sem):
        view = weight_view(item, block)
        return pltpu.make_async_remote_copy(
            src_ref=view,
            dst_ref=view,
            send_sem=send_sem.at[item],
            recv_sem=recv_sem.at[item],
            device_id={"tp": target},
            device_id_type=MESH,
        )

    far_copies, own_copies, fwd_copies = [], [], []
    for i in range(items):
        loads[i].wait()
        far_copies.append(weight_copy(i, tme, far, far_send, far_recv))
        far_copies[i].start()
        own_copies.append(weight_copy(i, tme, near, own_send, own_recv))
        own_copies[i].start()
        fwd_copies.append(weight_copy(i, far, near, fwd_send, fwd_recv))

    def far_arrival(item):
        return weight_copy(item, far, far, far_send, far_recv)

    def near_arrival(item):
        return weight_copy(item, near, near, own_send, own_recv)

    def near_far_arrival(item):
        return weight_copy(item, near_far, near, fwd_send, fwd_recv)

    normed = rms_scale(x_ref[...].astype(F32), x_gain_ref[...]).astype(BF16)
    expert_row = iota((ep, rows), 0)
    named_t = jnp.zeros((ep, rows), F32)
    for k in range(picks):
        named_t = named_t + jnp.where(routes_t_ref[k : k + 1, :] == expert_row, 1.0, 0.0)
    before_t = jnp.where(iota((rows, rows), 0) < iota((rows, rows), 1), 1.0, 0.0).astype(BF16)
    place_t = dot(named_t.astype(BF16), before_t) + (expert_row * slot_rows).astype(F32)
    slot_iota = iota((slots, rows), 0)
    pick_t = jnp.zeros((slots, rows), F32)
    for k in range(picks):
        slot_t = jnp.sum(
            jnp.where(routes_t_ref[k : k + 1, :] == expert_row, place_t, 0.0), axis=0, keepdims=True
        ).astype(jnp.int32)
        pick_t = pick_t + jnp.where(slot_iota == slot_t, 1.0, 0.0)
    pick_t = pick_t.astype(BF16)
    for c in range(chunks):
        send_x[:, :, c * cols : (c + 1) * cols] = (
            dot(pick_t, normed[:, c * cols : (c + 1) * cols])
            .astype(BF16)
            .reshape(ep, slot_rows, cols)
        )

    def x_copy(target, source):
        return pltpu.make_async_remote_copy(
            src_ref=send_x.at[target, pl.ds(0, wire_rows)],
            dst_ref=recv_x.at[source, pl.ds(0, wire_rows)],
            send_sem=x_send_sem.at[target],
            recv_sem=x_recv_sem.at[source],
            device_id={"ep": target},
            device_id_type=MESH,
        )

    def kv_copy(target, source):
        return pltpu.make_async_remote_copy(
            src_ref=kv_ref,
            dst_ref=kv_all.at[source],
            send_sem=kv_send_sem.at[target],
            recv_sem=kv_recv_sem.at[source],
            device_id={"ep": target},
            device_id_type=MESH,
        )

    def over_peers(action):
        def step_of(step, carry):
            action(lax.rem(me + step, ep))
            return carry

        lax.fori_loop(1, ep, step_of, 0)

    over_peers(lambda peer: x_copy(peer, me).start())

    def kv_start(peer, carry):
        kv_copy(peer, me).start()
        return carry

    lax.fori_loop(me + 1, ep, kv_start, 0)
    recv_x[me] = send_x[me]
    kv_all[me] = kv_ref[...]

    expert_col = iota((rows, ep), 1)
    named = jnp.zeros((rows, ep), F32)
    for k in range(picks):
        named = named + jnp.where(routes_ref[:, k : k + 1] == expert_col, 1.0, 0.0)
    before = jnp.where(iota((rows, rows), 0) > iota((rows, rows), 1), 1.0, 0.0).astype(BF16)
    place = dot(before, named.astype(BF16)) + (expert_col * slot_rows).astype(F32)
    slot_of = [
        jnp.sum(
            jnp.where(routes_ref[:, k : k + 1] == expert_col, place, 0.0), axis=1, keepdims=True
        ).astype(jnp.int32)
        for k in range(picks)
    ]
    for h in range(heads):
        select = jnp.where(
            (iota((heads * HEAD, 2 * HEAD), 0) == iota((heads * HEAD, 2 * HEAD), 1) + h * HEAD)
            & (iota((heads * HEAD, 2 * HEAD), 1) < HEAD),
            1.0,
            0.0,
        ).astype(BF16)
        q_pad[h] = dot(q_ref[...], select).astype(BF16)
    top[...] = jnp.full(top.shape, NEGATIVE, F32)
    total[...] = jnp.zeros_like(total)
    summed[...] = jnp.zeros_like(summed)

    for i in range(2):
        far_arrival(i).wait_recv()
        fwd_copies[i].start()
    for i in range(2):
        near_arrival(i).wait_recv()
        near_far_arrival(i).wait_recv()
    over_peers(lambda peer: x_copy(me, peer).wait_recv())

    def hidden_block(block, carry):
        taken = recv_x[...].reshape(slots, width)
        gated = dot(taken, gate_all[block])
        lifted = dot(taken, up_all[block])
        hidden[:, pl.ds(pl.multiple_of(block * shard, shard), shard)] = (
            gated / (1.0 + jnp.exp(-gated)) * lifted
        ).astype(BF16)
        return carry

    lax.fori_loop(0, tp, hidden_block, 0)
    for i in range(2, items):
        far_arrival(i).wait_recv()
        fwd_copies[i].start()

    def y_copy(c, target, source):
        return pltpu.make_async_remote_copy(
            src_ref=send_y.at[c, target, pl.ds(0, wire_rows)],
            dst_ref=recv_y.at[c, source, pl.ds(0, wire_rows)],
            send_sem=y_send_sem.at[c, target],
            recv_sem=y_recv_sem.at[c, source],
            device_id={"ep": target},
            device_id_type=MESH,
        )

    for c in range(chunks):
        near_arrival(2 + c).wait_recv()
        near_far_arrival(2 + c).wait_recv()
        send_y[c] = dot(hidden[...], down_all[c]).astype(BF16).reshape(ep, slot_rows, cols)
        over_peers(lambda peer: y_copy(c, peer, me).start())
        recv_y[c, me] = send_y[c, me]

    def key_block(block, carry):
        @pl.when(block < me)
        def _():
            kv_copy(me, block).wait_recv()

        causal = block * tokens + iota((tokens, tokens), 1) <= me * tokens + iota(
            (tokens, tokens), 0
        )
        for h in range(heads):
            pair = kv_all[block, :, (h // group) * 2 * HEAD : (h // group + 1) * 2 * HEAD]
            scores = (
                lax.dot_general(
                    q_pad[h], pair, (((1,), (1,)), ((), ())), preferred_element_type=F32
                )
                * HEAD ** (-0.5)
            )
            scores = scores + query_gate_ref[:, h : h + 1] - key_gate_ref[block, h : h + 1, :]
            scores = jnp.where(causal, scores, NEGATIVE)
            old = top[h]
            new = jnp.maximum(old, jnp.max(scores, axis=-1, keepdims=True))
            factor = jnp.exp(old - new)
            weight = jnp.where(causal, jnp.exp(scores - new[:, :1]), 0.0)
            top[h] = new
            total[h] = total[h] * factor + jnp.sum(weight, axis=-1, keepdims=True)
            summed[h] = summed[h] * factor + dot(weight.astype(BF16), pair)
        return carry

    lax.fori_loop(0, me + 1, key_block, 0)
    attended = jnp.zeros((tokens, heads * HEAD), F32)
    for h in range(heads):
        part = (summed[h] / total[h]).astype(BF16)
        select = jnp.where(
            (iota((2 * HEAD, heads * HEAD), 0) + (h - 1) * HEAD == iota((2 * HEAD, heads * HEAD), 1))
            & (iota((2 * HEAD, heads * HEAD), 0) >= HEAD),
            1.0,
            0.0,
        ).astype(BF16)
        attended = attended + dot(part, select)
    attended = attended.astype(BF16)
    for c in range(chunks):
        mix_send[:, :, c * cols : (c + 1) * cols] = (
            dot(attended, mixw_ref[:, c * cols : (c + 1) * cols])
            .astype(BF16)
            .reshape(tp, tokens // tp, cols)
        )

    def mix_copy(target, source):
        return pltpu.make_async_remote_copy(
            src_ref=mix_send.at[target],
            dst_ref=mix_recv.at[source],
            send_sem=mix_send_sem.at[target],
            recv_sem=mix_recv_sem.at[source],
            device_id={"tp": target},
            device_id_type=MESH,
        )

    for step in range(1, tp):
        mix_copy(lax.rem(tme + step, tp), tme).start()
    mix_recv[tme] = mix_send[tme]
    for step in range(1, tp):
        mix_copy(tme, lax.rem(tme + step, tp)).wait_recv()
    mixed = mix_recv[0].astype(F32)
    for j in range(1, tp):
        mixed = mixed + mix_recv[j].astype(F32)
    mix_out[...] = rms_scale(mixed, mix_gain_ref[...]).astype(BF16)

    slot_lane = iota((rows, slots), 1)
    for c in range(chunks):
        over_peers(lambda peer: y_copy(c, me, peer).wait_recv())
        back = recv_y[c].reshape(slots, cols)
        blend = jnp.zeros((rows, cols), F32)
        for k in range(picks):
            pick = jnp.where(slot_lane == slot_of[k], 1.0, 0.0).astype(BF16)
            blend = blend + route_weight_ref[:, k : k + 1] * dot(pick, back)
        moe_out[:, c * cols : (c + 1) * cols] = blend.astype(BF16)

    for i in range(items):
        far_copies[i].wait_send()
        own_copies[i].wait_send()
        fwd_copies[i].wait_send()
    over_peers(lambda peer: x_copy(peer, me).wait_send())

    def kv_end(peer, carry):
        kv_copy(peer, me).wait_send()
        return carry

    lax.fori_loop(me + 1, ep, kv_end, 0)
    for c in range(chunks):
        over_peers(lambda peer: y_copy(c, peer, me).wait_send())
    for step in range(1, tp):
        mix_copy(lax.rem(tme + step, tp), tme).wait_send()


def body(
    queries,
    keys_values,
    log_gate_cum,
    mix_weight,
    mix_gain,
    moe_in,
    moe_gain,
    routes,
    route_weight,
    expert_gate,
    expert_up,
    expert_down,
):
    ep, tp = lax.axis_size("ep"), lax.axis_size("tp")
    me = lax.axis_index("ep")
    tokens = queries.shape[0]
    heads = log_gate_cum.shape[0]
    rows, width = moe_in.shape
    picks = routes.shape[1]
    capacity = 3 * picks * rows // (2 * ep)
    slot_rows, wire_rows = round_up(capacity, 16), round_up(capacity, WIRE)
    chunks = 4
    cols = width // chunks
    depth, shard = expert_gate.shape[1:]
    key_gate = jnp.transpose(log_gate_cum.reshape(heads, ep, tokens), (1, 0, 2))
    query_gate = lax.dynamic_slice_in_dim(log_gate_cum, me * tokens, tokens, 1).T
    vmem = pl.BlockSpec(memory_space=pltpu.VMEM)
    hbm = pl.BlockSpec(memory_space=pl.ANY)
    dma = pltpu.SemaphoreType.DMA
    items = 2 + chunks
    return pl.pallas_call(
        partial(kernel, (ep, tp, slot_rows, wire_rows, chunks)),
        out_shape=(
            jax.ShapeDtypeStruct((tokens // tp, width), BF16),
            jax.ShapeDtypeStruct((rows, width), BF16),
        ),
        in_specs=[vmem] * 11 + [hbm] * 3,
        out_specs=(vmem, vmem),
        scratch_shapes=[
            pltpu.VMEM((tp, depth, shard), BF16),
            pltpu.VMEM((tp, depth, shard), BF16),
            pltpu.VMEM((chunks, tp * shard, cols), BF16),
            pltpu.VMEM((ep, slot_rows, width), BF16),
            pltpu.VMEM((ep, slot_rows, width), BF16),
            pltpu.VMEM((ep * slot_rows, tp * shard), BF16),
            pltpu.VMEM((chunks, ep, slot_rows, cols), BF16),
            pltpu.VMEM((chunks, ep, slot_rows, cols), BF16),
            pltpu.VMEM((ep,) + keys_values.shape, BF16),
            pltpu.VMEM((heads, tokens, 2 * HEAD), BF16),
            pltpu.VMEM((heads, tokens, 2 * HEAD), F32),
            pltpu.VMEM((heads, tokens, 2 * HEAD), F32),
            pltpu.VMEM((heads, tokens, 2 * HEAD), F32),
            pltpu.VMEM((tp, tokens // tp, width), BF16),
            pltpu.VMEM((tp, tokens // tp, width), BF16),
        ]
        + [dma((items,))] * 7
        + [dma((ep,))] * 4
        + [dma((chunks, ep))] * 2
        + [dma((tp,))] * 2,
        compiler_params=pltpu.CompilerParams(
            collective_id=0, has_side_effects=True, vmem_limit_bytes=60 * 1024 * 1024
        ),
    )(
        queries,
        keys_values,
        key_gate,
        query_gate,
        mix_weight,
        mix_gain.reshape(1, -1),
        moe_in,
        moe_gain.reshape(1, -1),
        routes,
        routes.T,
        route_weight,
        expert_gate,
        expert_up,
        expert_down,
    )


WIRE = 8


def solution(mesh):
    in_specs = (
        P("ep", "tp"),
        P("ep", "tp"),
        P("tp", None),
        P("tp", None),
        P(),
        P(("ep", "tp"), None),
        P(),
        P(("ep", "tp"), None),
        P(("ep", "tp"), None),
        P("ep", None, "tp"),
        P("ep", None, "tp"),
        P("ep", "tp", None),
    )
    out_specs = (P(("ep", "tp"), None), P(("ep", "tp"), None))
    return jax.shard_map(body, mesh=mesh, in_specs=in_specs, out_specs=out_specs, check_vma=False)
```

time: 232 us -> 138 us (0.59)
  Pallas kernels: 0 us -> 129 us
  blocking collectives: 72.5 us -> 0 us
  waiting for transfers between devices: 50.7 us -> 0 us
  local copies, waits for them, and re-layouts: 37.5 us -> 6.79 us
  matrix products: 23.2 us -> 0 us
  other arithmetic: 19.6 us -> 0 us
  between operations: 14 us -> 0.65 us
  starting transfers between devices: 13.2 us -> 0 us
    pallas_call x0 -> x1, Pallas kernels: none -> 129 us  [body(): pl.pallas_call(partial(kernel, (ep, tp, slot_rows, wire_rows, chunks)), o...]
    all_gather x1 -> x0, blocking collectives: 72.5 us -> none  [body(): piece = lax.all_gather(keys_values, 'ep', axis=0, tiled=True)]
    reduce_scatter x1 -> x0, waiting for transfers between devices: 45.4 us -> none  [body(): lax.psum_scatter(jnp.dot(attended, mix_weight, preferred_element_type=jnp...]
    dot_general x11 -> x0, matrix products: 23.2 us -> none  [the longest x1 6.42 us: gated_hidden(): jnp.dot(slot_rows, up_columns, preferred_element_type=jnp.float32)]
    all_to_all x2 -> x0, starting transfers between devices: 12.8 us -> none  [the longest x1 7.28 us: body(): lax.all_to_all(padded[source_row].reshape(ep_count, capacity, width_here)...]
    reduce_sum x6 -> x0, other arithmetic: 9.61 us -> none  [the longest x1 7.76 us: body(): jnp.sum(route_weight[..., None] * chosen, axis=1).astype(jnp.bfloat16)]
    dynamic_slice x9 -> x1, local copies, waits for them, and re-layouts: 10.2 us -> 0.69 us  [body(): lax.dynamic_slice_in_dim(log_gate_cum, me * tokens, tokens, 1)]
    gather x2 -> x0, local copies, waits for them, and re-layouts: 7.16 us -> none  [the longest x1 4.04 us: body(): padded[source_row].reshape(ep_count, capacity, width_here)]
  transfers between devices with their start and end apart: 6 -> 0, of which waited for: 2 -> 0; matrix products, arithmetic and copies ran while one was open for 23% -> 0% of each run, Pallas kernels for 0% -> 0%
where the time goes in v1:
time: 138 us; the launch traced here: 137 us
  Pallas kernels  129 us (93%)
  local copies, waits for them, and re-layouts  6.79 us (5%)
    pallas_call x1, Pallas kernels, body(): pl.pallas_call(partial(kernel, (ep, tp, slot_rows, wire_rows, chunks)), o...  129 us
    unnamed x9, local copies, waits for them, and re-layouts  6.1 us

profile of v1, /device:TPU:0, one launch (start us, length us, event | category | flops | bytes accessed | tf_op | source)
XLA Modules:
  0.0 136.8 jit_solution(15371429305161548317)
XLA Ops:
  0.6 0.0 copy-start.1
  0.6 0.7 constant_dynamic-slice_fusion
  1.3 0.0 copy-done.1
  1.3 0.0 copy-start
  1.3 0.8 copy.16.route_weight_ref
  2.1 0.0 copy-done
  2.1 0.8 copy.15.routes_ref
  2.9 0.8 copy.17
  3.7 129.3 %shard_map.131 = (bf16[64,2048]{1,0:T(8,128)(2,1)}, bf16[192,2048]{1,0:T(8,128)(2,1)}) custom-call(bf16[256,256]{1,0:T(8,128)(2,1)} %q_ref.1, bf16[256,128]{1,0:T(8,128)(2,1)} %kv_ref.1, f32[8,4,256]{2,1,0:T(4,128)} %bitcast.8, f32[256,4]{1,0:T(8,128)} %bitcast.7, bf16[256,2048]{1,0:T(8,128)(2,1)} %mixw_ref.1, f32[1,2048]{1,0:T(1,128)} %bitcast.10, ...), custom_call_target="tpu_custom_call" | custom-call | tf_op jit(solution)/shard_map/pallas_call | solution.py:413
  133.0 1.7 %copy.20 = bf16[64,2048]{1,0:T(8,128)(2,1)} copy(bf16[64,2048]{1,0:T(8,128)(2,1)} %get-tuple-element.4) | data formatting | bytes 524288
  134.7 2.1 %copy.21 = bf16[192,2048]{1,0:T(8,128)(2,1)} copy(bf16[192,2048]{1,0:T(8,128)(2,1)} %get-tuple-element.5) | data formatting | bytes 1572864
Async XLA Ops:
  0.6 0.7 copy-start.1
  1.3 0.8 copy-start

commit v2 on v1

--- a/solution.py
+++ b/solution.py
@@ -36,14 +36,12 @@
     q_ref,
     kv_ref,
     key_gate_ref,
-    query_gate_ref,
     mixw_ref,
     mix_gain_ref,
     x_ref,
     x_gain_ref,
-    routes_ref,
     routes_t_ref,
-    route_weight_ref,
+    route_weight_t_ref,
     gate_hbm,
     up_hbm,
     down_hbm,
@@ -52,6 +50,8 @@
     gate_all,
     up_all,
     down_all,
+    pick_all,
+    normed_all,
     send_x,
     recv_x,
     hidden,
@@ -59,6 +59,7 @@
     recv_y,
     kv_all,
     q_pad,
+    query_gate,
     top,
     total,
     summed,
@@ -87,12 +88,16 @@
     near = tme + 1 - 2 * lax.rem(tme, 2)
     near_far = lax.rem(near + tp // 2, tp)
     rows, width = x_ref.shape
-    picks = routes_ref.shape[1]
+    picks = routes_t_ref.shape[0]
     slots = ep * slot_rows
     shard = down_hbm.shape[1]
     cols = width // chunks
     tokens = q_ref.shape[0]
-    heads = query_gate_ref.shape[1]
+    heads = key_gate_ref.shape[1]
+    half = ep // 2
+    own_start = (me // half) * half
+    cross_start = half - own_start
+    turn = me - own_start
     kv_local = kv_ref.shape[1] // (2 * HEAD)
     group = heads // kv_local
 
@@ -133,6 +138,25 @@
         pl.semaphore_signal(
             barrier, inc=1, device_id={"tp": lax.rem(tme + step, tp)}, device_id_type=MESH
         )
+    normed = rms_scale(x_ref[...].astype(F32), x_gain_ref[...]).astype(BF16)
+    expert_row = iota((ep, rows), 0)
+    named_t = jnp.zeros((ep, rows), F32)
+    for k in range(picks):
+        named_t = named_t + jnp.where(routes_t_ref[k : k + 1, :] == expert_row, 1.0, 0.0)
+    before_t = jnp.where(iota((rows, rows), 0) < iota((rows, rows), 1), 1.0, 0.0).astype(BF16)
+    place_t = dot(named_t.astype(BF16), before_t) + (expert_row * slot_rows).astype(F32)
+    slot_iota = iota((slots, rows), 0)
+    pick_t = jnp.zeros((slots, rows), F32)
+    slot_rows_of = []
+    for k in range(picks):
+        slot_t = jnp.sum(
+            jnp.where(routes_t_ref[k : k + 1, :] == expert_row, place_t, 0.0), axis=0, keepdims=True
+        )
+        slot_rows_of.append(slot_t)
+        pick_t = pick_t + jnp.where(slot_iota == slot_t.astype(jnp.int32), 1.0, 0.0)
+    pick_all[...] = pick_t.astype(BF16).reshape(ep, slot_rows, rows)
+    normed_all[...] = normed
+
     pl.semaphore_wait(barrier, ep - 1 + tp - 1)
 
     def weight_copy(item, block, target, send_sem, recv_sem):
@@ -164,28 +188,6 @@
     def near_far_arrival(item):
         return weight_copy(item, near_far, near, fwd_send, fwd_recv)
 
-    normed = rms_scale(x_ref[...].astype(F32), x_gain_ref[...]).astype(BF16)
-    expert_row = iota((ep, rows), 0)
-    named_t = jnp.zeros((ep, rows), F32)
-    for k in range(picks):
-        named_t = named_t + jnp.where(routes_t_ref[k : k + 1, :] == expert_row, 1.0, 0.0)
-    before_t = jnp.where(iota((rows, rows), 0) < iota((rows, rows), 1), 1.0, 0.0).astype(BF16)
-    place_t = dot(named_t.astype(BF16), before_t) + (expert_row * slot_rows).astype(F32)
-    slot_iota = iota((slots, rows), 0)
-    pick_t = jnp.zeros((slots, rows), F32)
-    for k in range(picks):
-        slot_t = jnp.sum(
-            jnp.where(routes_t_ref[k : k + 1, :] == expert_row, place_t, 0.0), axis=0, keepdims=True
-        ).astype(jnp.int32)
-        pick_t = pick_t + jnp.where(slot_iota == slot_t, 1.0, 0.0)
-    pick_t = pick_t.astype(BF16)
-    for c in range(chunks):
-        send_x[:, :, c * cols : (c + 1) * cols] = (
-            dot(pick_t, normed[:, c * cols : (c + 1) * cols])
-            .astype(BF16)
-            .reshape(ep, slot_rows, cols)
-        )
-
     def x_copy(target, source):
         return pltpu.make_async_remote_copy(
             src_ref=send_x.at[target, pl.ds(0, wire_rows)],
@@ -213,28 +215,45 @@
 
         lax.fori_loop(1, ep, step_of, 0)
 
-    over_peers(lambda peer: x_copy(peer, me).start())
+    def over_half(start, first, action):
+        def step_of(step, carry):
+            action(start + lax.rem(turn + step, half))
+            return carry
+
+        lax.fori_loop(first, half, step_of, 0)
+
+    def fill(peer):
+        return dot(pick_all[peer], normed_all[...]).astype(BF16)
+
+    def dispatch(peer):
+        send_x[peer] = fill(peer)
+        x_copy(peer, me).start()
+
+    def dispatch_pair(step, carry):
+        dispatch(cross_start + lax.rem(turn + step, half))
+
+        @pl.when(step > 0)
+        def _():
+            dispatch(own_start + lax.rem(turn + step, half))
+
+        return carry
+
+    lax.fori_loop(0, half, dispatch_pair, 0)
 
     def kv_start(peer, carry):
         kv_copy(peer, me).start()
         return carry
 
     lax.fori_loop(me + 1, ep, kv_start, 0)
-    recv_x[me] = send_x[me]
+    recv_x[me] = fill(me)
     kv_all[me] = kv_ref[...]
 
-    expert_col = iota((rows, ep), 1)
-    named = jnp.zeros((rows, ep), F32)
-    for k in range(picks):
-        named = named + jnp.where(routes_ref[:, k : k + 1] == expert_col, 1.0, 0.0)
-    before = jnp.where(iota((rows, rows), 0) > iota((rows, rows), 1), 1.0, 0.0).astype(BF16)
-    place = dot(before, named.astype(BF16)) + (expert_col * slot_rows).astype(F32)
-    slot_of = [
-        jnp.sum(
-            jnp.where(routes_ref[:, k : k + 1] == expert_col, place, 0.0), axis=1, keepdims=True
-        ).astype(jnp.int32)
-        for k in range(picks)
-    ]
+    def column(row):
+        size = row.shape[1]
+        same = iota((size, size), 0) == iota((size, size), 1)
+        return jnp.sum(jnp.where(same, row, 0.0), axis=1, keepdims=True)
+
+    slot_of = [column(row).astype(jnp.int32) for row in slot_rows_of]
     for h in range(heads):
         select = jnp.where(
             (iota((heads * HEAD, 2 * HEAD), 0) == iota((heads * HEAD, 2 * HEAD), 1) + h * HEAD)
@@ -243,6 +262,7 @@
             0.0,
         ).astype(BF16)
         q_pad[h] = dot(q_ref[...], select).astype(BF16)
+        query_gate[h] = column(key_gate_ref[me, h : h + 1, :])
     top[...] = jnp.full(top.shape, NEGATIVE, F32)
     total[...] = jnp.zeros_like(total)
     summed[...] = jnp.zeros_like(summed)
@@ -253,21 +273,25 @@
     for i in range(2):
         near_arrival(i).wait_recv()
         near_far_arrival(i).wait_recv()
-    over_peers(lambda peer: x_copy(me, peer).wait_recv())
-
-    def hidden_block(block, carry):
-        taken = recv_x[...].reshape(slots, width)
-        gated = dot(taken, gate_all[block])
-        lifted = dot(taken, up_all[block])
-        hidden[:, pl.ds(pl.multiple_of(block * shard, shard), shard)] = (
-            gated / (1.0 + jnp.exp(-gated)) * lifted
-        ).astype(BF16)
-        return carry
-
-    lax.fori_loop(0, tp, hidden_block, 0)
-    for i in range(2, items):
-        far_arrival(i).wait_recv()
-        fwd_copies[i].start()
+
+    def hidden_half(start, index):
+        def hidden_block(block, carry):
+            taken = recv_x[pl.ds(start, half)].reshape(half * slot_rows, width)
+            gated = dot(taken, gate_all[block])
+            lifted = dot(taken, up_all[block])
+            hidden[index, :, pl.ds(pl.multiple_of(block * shard, shard), shard)] = (
+                gated / (1.0 + jnp.exp(-gated)) * lifted
+            ).astype(BF16)
+            return carry
+
+        lax.fori_loop(0, tp, hidden_block, 0)
+
+    over_half(own_start, 1, lambda peer: x_copy(me, peer).wait_recv())
+    hidden_half(own_start, 0)
+    far_arrival(2).wait_recv()
+    fwd_copies[2].start()
+    over_half(cross_start, 0, lambda peer: x_copy(me, peer).wait_recv())
+    hidden_half(cross_start, 1)
 
     def y_copy(c, target, source):
         return pltpu.make_async_remote_copy(
@@ -279,11 +303,22 @@
             device_id_type=MESH,
         )
 
+    def results(c, start, index):
+        send_y[c, pl.ds(start, half)] = (
+            dot(hidden[index], down_all[c]).astype(BF16).reshape(half, slot_rows, cols)
+        )
+
     for c in range(chunks):
+        if c > 0:
+            far_arrival(2 + c).wait_recv()
+            fwd_copies[2 + c].start()
         near_arrival(2 + c).wait_recv()
         near_far_arrival(2 + c).wait_recv()
-        send_y[c] = dot(hidden[...], down_all[c]).astype(BF16).reshape(ep, slot_rows, cols)
-        over_peers(lambda peer: y_copy(c, peer, me).start())
+        results(c, cross_start, 1)
+        over_half(cross_start, 0, lambda peer: y_copy(c, peer, me).start())
+    for c in range(chunks):
+        results(c, own_start, 0)
+        over_half(own_start, 1, lambda peer: y_copy(c, peer, me).start())
         recv_y[c, me] = send_y[c, me]
 
     def key_block(block, carry):
@@ -302,7 +337,7 @@
                 )
                 * HEAD ** (-0.5)
             )
-            scores = scores + query_gate_ref[:, h : h + 1] - key_gate_ref[block, h : h + 1, :]
+            scores = scores + query_gate[h] - key_gate_ref[block, h : h + 1, :]
             scores = jnp.where(causal, scores, NEGATIVE)
             old = top[h]
             new = jnp.maximum(old, jnp.max(scores, axis=-1, keepdims=True))
@@ -353,13 +388,14 @@
     mix_out[...] = rms_scale(mixed, mix_gain_ref[...]).astype(BF16)
 
     slot_lane = iota((rows, slots), 1)
+    scale_of = [column(route_weight_t_ref[k : k + 1, :]) for k in range(picks)]
     for c in range(chunks):
         over_peers(lambda peer: y_copy(c, me, peer).wait_recv())
         back = recv_y[c].reshape(slots, cols)
         blend = jnp.zeros((rows, cols), F32)
         for k in range(picks):
             pick = jnp.where(slot_lane == slot_of[k], 1.0, 0.0).astype(BF16)
-            blend = blend + route_weight_ref[:, k : k + 1] * dot(pick, back)
+            blend = blend + scale_of[k] * dot(pick, back)
         moe_out[:, c * cols : (c + 1) * cols] = blend.astype(BF16)
 
     for i in range(items):
@@ -377,6 +413,11 @@
         over_peers(lambda peer: y_copy(c, peer, me).wait_send())
     for step in range(1, tp):
         mix_copy(lax.rem(tme + step, tp), tme).wait_send()
+
+
+def copy_kernel(mix_in, moe_in, mix_out, moe_out):
+    mix_out[...] = mix_in[...]
+    moe_out[...] = moe_in[...]
 
 
 def body(
@@ -394,7 +435,6 @@
     expert_down,
 ):
     ep, tp = lax.axis_size("ep"), lax.axis_size("tp")
-    me = lax.axis_index("ep")
     tokens = queries.shape[0]
     heads = log_gate_cum.shape[0]
     rows, width = moe_in.shape
@@ -405,30 +445,32 @@
     cols = width // chunks
     depth, shard = expert_gate.shape[1:]
     key_gate = jnp.transpose(log_gate_cum.reshape(heads, ep, tokens), (1, 0, 2))
-    query_gate = lax.dynamic_slice_in_dim(log_gate_cum, me * tokens, tokens, 1).T
     vmem = pl.BlockSpec(memory_space=pltpu.VMEM)
     hbm = pl.BlockSpec(memory_space=pl.ANY)
     dma = pltpu.SemaphoreType.DMA
     items = 2 + chunks
-    return pl.pallas_call(
+    results = pl.pallas_call(
         partial(kernel, (ep, tp, slot_rows, wire_rows, chunks)),
         out_shape=(
             jax.ShapeDtypeStruct((tokens // tp, width), BF16),
             jax.ShapeDtypeStruct((rows, width), BF16),
         ),
-        in_specs=[vmem] * 11 + [hbm] * 3,
+        in_specs=[vmem] * 9 + [hbm] * 3,
         out_specs=(vmem, vmem),
         scratch_shapes=[
             pltpu.VMEM((tp, depth, shard), BF16),
             pltpu.VMEM((tp, depth, shard), BF16),
             pltpu.VMEM((chunks, tp * shard, cols), BF16),
+            pltpu.VMEM((ep, slot_rows, rows), BF16),
+            pltpu.VMEM((rows, width), BF16),
             pltpu.VMEM((ep, slot_rows, width), BF16),
             pltpu.VMEM((ep, slot_rows, width), BF16),
-            pltpu.VMEM((ep * slot_rows, tp * shard), BF16),
+            pltpu.VMEM((2, ep // 2 * slot_rows, tp * shard), BF16),
             pltpu.VMEM((chunks, ep, slot_rows, cols), BF16),
             pltpu.VMEM((chunks, ep, slot_rows, cols), BF16),
             pltpu.VMEM((ep,) + keys_values.shape, BF16),
             pltpu.VMEM((heads, tokens, 2 * HEAD), BF16),
+            pltpu.VMEM((heads, tokens, 1), F32),
             pltpu.VMEM((heads, tokens, 2 * HEAD), F32),
             pltpu.VMEM((heads, tokens, 2 * HEAD), F32),
             pltpu.VMEM((heads, tokens, 2 * HEAD), F32),
@@ -446,18 +488,23 @@
         queries,
         keys_values,
         key_gate,
-        query_gate,
         mix_weight,
         mix_gain.reshape(1, -1),
         moe_in,
         moe_gain.reshape(1, -1),
-        routes,
         routes.T,
-        route_weight,
+        route_weight.T,
         expert_gate,
         expert_up,
         expert_down,
     )
+
+    return pl.pallas_call(
+        copy_kernel,
+        out_shape=tuple(jax.ShapeDtypeStruct(r.shape, r.dtype) for r in results),
+        in_specs=[vmem] * 2,
+        out_specs=(vmem, vmem),
+    )(*results)
 
 
 WIRE = 8

time: 138 us -> 127 us (0.920)
  local copies, waits for them, and re-layouts: 6.79 us -> 0 us
  Pallas kernels: 129 us -> 125 us
    pallas_call x1, Pallas kernels: 129 us -> 122 us  [body(): pl.pallas_call(partial(kernel, (ep, tp, slot_rows, wire_rows, chunks)), o...]
    unnamed x9 -> x0, local copies, waits for them, and re-layouts: 6.1 us -> none
    pallas_call x0 -> x1, Pallas kernels: none -> 2.2 us  [body(): pl.pallas_call(copy_kernel, out_shape=tuple((jax.ShapeDtypeStruct(r.shape...]
where the time goes in v2:
time: 127 us; the launch traced here: 125 us
  Pallas kernels  125 us (98%)
    pallas_call x1, Pallas kernels, body(): pl.pallas_call(partial(kernel, (ep, tp, slot_rows, wire_rows, chunks)), o...  122 us

profile of v2, /device:TPU:0, one launch (start us, length us, event | category | flops | bytes accessed | tf_op | source)
XLA Modules:
  0.0 125.2 jit_solution(13845169968110038055)
XLA Ops:
  0.6 122.4 %shard_map.131 = (bf16[64,2048]{1,0:T(8,128)(2,1)}, bf16[192,2048]{1,0:T(8,128)(2,1)}) custom-call(bf16[256,256]{1,0:T(8,128)(2,1)} %q_ref.1, bf16[256,128]{1,0:T(8,128)(2,1)} %kv_ref.1, f32[8,4,256]{2,1,0:T(4,128)} %bitcast.7, bf16[256,2048]{1,0:T(8,128)(2,1)} %mixw_ref.1, f32[1,2048]{1,0:T(1,128)} %bitcast.8, bf16[192,2048]{1,0:T(8,128)(2,1)} %x_ref.1, ...), custom_call_target="tpu_custom_call" | custom-call | tf_op jit(solution)/shard_map/pallas_call | solution.py:452
  123.0 2.2 %shard_map.132 = (bf16[64,2048]{1,0:T(8,128)(2,1)}, bf16[192,2048]{1,0:T(8,128)(2,1)}) custom-call(bf16[64,2048]{1,0:T(8,128)(2,1)} %get-tuple-element.4.mix_in, bf16[192,2048]{1,0:T(8,128)(2,1)} %get-tuple-element.5.moe_in), custom_call_target="tpu_custom_call" | custom-call | tf_op jit(solution)/shard_map/pallas_call | solution.py:502

commit v3 on v2

--- a/solution.py
+++ b/solution.py
@@ -441,7 +441,7 @@
     picks = routes.shape[1]
     capacity = 3 * picks * rows // (2 * ep)
     slot_rows, wire_rows = round_up(capacity, 16), round_up(capacity, WIRE)
-    chunks = 4
+    chunks = 8
     cols = width // chunks
     depth, shard = expert_gate.shape[1:]
     key_gate = jnp.transpose(log_gate_cum.reshape(heads, ep, tokens), (1, 0, 2))

time: 127 us -> 147 us (1.16)
  the two profiles are of different devices: /device:TPU:0 before, /device:TPU:25 now
where the time goes in v3:
time: 147 us; the launch traced here: 146 us
  Pallas kernels  146 us (99%)
    pallas_call x1, Pallas kernels, body(): pl.pallas_call(partial(kernel, (ep, tp, slot_rows, wire_rows, chunks)), o...  144 us

profile of v3, /device:TPU:25, one launch (start us, length us, event | category | flops | bytes accessed | tf_op | source)
XLA Modules:
  0.0 146.3 jit_solution(1736917279604100837)
XLA Ops:
  0.6 143.5 %shard_map.131 = (bf16[64,2048]{1,0:T(8,128)(2,1)}, bf16[192,2048]{1,0:T(8,128)(2,1)}) custom-call(bf16[256,256]{1,0:T(8,128)(2,1)} %q_ref.1, bf16[256,128]{1,0:T(8,128)(2,1)} %kv_ref.1, f32[8,4,256]{2,1,0:T(4,128)} %bitcast.7, bf16[256,2048]{1,0:T(8,128)(2,1)} %mixw_ref.1, f32[1,2048]{1,0:T(1,128)} %bitcast.8, bf16[192,2048]{1,0:T(8,128)(2,1)} %x_ref.1, ...), custom_call_target="tpu_custom_call" | custom-call | tf_op jit(solution)/shard_map/pallas_call | solution.py:452
  144.1 2.2 %shard_map.132 = (bf16[64,2048]{1,0:T(8,128)(2,1)}, bf16[192,2048]{1,0:T(8,128)(2,1)}) custom-call(bf16[64,2048]{1,0:T(8,128)(2,1)} %get-tuple-element.4.mix_in, bf16[192,2048]{1,0:T(8,128)(2,1)} %get-tuple-element.5.moe_in), custom_call_target="tpu_custom_call" | custom-call | tf_op jit(solution)/shard_map/pallas_call | solution.py:502
